TPU v7x, 32 devices: a whole 2x2x4 slice. The times are simulated.
32 devices in a mesh: grp: 2 (over y), fs: 4 (over z), tp: 4 (over x, core).
Axes of the slice: x: 2, y: 2, z: 4, core: 2. Of those that a mesh axis runs over, the one named last changes fastest.
Arguments:
- tokens: bfloat16 [8, 384, 2048], P(('grp', 'fs'), None, 'tp'), parts along dimension 0, may hold values from -24 to 24
- input_gain: float32 [2048], replicated, may hold values from 0.1 to 1.9
- query_weight: bfloat16 [2048, 1024], P('fs', 'tp'), may hold values from -0.125 to 0.125
- key_weight: bfloat16 [2048, 1024], P('fs', 'tp'), may hold values from -0.125 to 0.125
- value_weight: bfloat16 [2048, 1024], P('fs', 'tp'), may hold values from -0.125 to 0.125
- output_gate_matrix: bfloat16 [2048, 1024], P('fs', 'tp'), may hold values from -0.125 to 0.125
- forward_decay: float32 [16], P('tp'), may hold values from -1 to 9
- backward_decay: float32 [16], P('tp'), may hold values from -1 to 9
- merge_weight: bfloat16 [1024, 2048], P('tp', 'fs'), may hold values from -0.375 to 0.375
- middle_gain: float32 [2048], replicated, may hold values from 0.1 to 1.9
- gate_weight: bfloat16 [2048, 5120], P('fs', 'tp'), may hold values from -0.125 to 0.125
- up_weight: bfloat16 [2048, 5120], P('fs', 'tp'), may hold values from -0.125 to 0.125
- down_weight: bfloat16 [5120, 2048], P('tp', 'fs'), may hold values from -0.15625 to 0.15625
Outputs:
- layer_out: bfloat16 [8, 384, 2048], P(('grp', 'fs'), None, 'tp'), parts along dimension 0
There are 2 independent parts, one for each index of `grp`. A program takes and returns all parts, laid end to end along the dimension named above; an argument that names none is the same for every part. Nothing has to cross between parts.
All inputs are finite; a program needn't handle non-finite values.
Results may differ from a plain program's by a relative error of at most 0.019.
Values may be sent and summed in bfloat16 or wider, within the bound.
A program may use at most 64 MiB of HBM per device.

v0:
```python
import jax
import jax.numpy as jnp
from jax import lax
from jax.sharding import PartitionSpec as P

BLOCK = 128


norm_eps = 1e-06
group_eps = 1e-05
rope_base = 10000.0
highest_precision = lax.Precision.HIGHEST


def rms_scale(values, gain_vector):
    widened = values.astype(jnp.float32)
    scaled = widened * lax.rsqrt(jnp.mean(widened * widened, axis=-1, keepdims=True) + norm_eps)
    return (scaled * gain_vector).astype(jnp.bfloat16)


def apply_rotary_heads(values, length):
    half_dim = values.shape[-1] // 2
    inverse = rope_base ** (-jnp.arange(half_dim, dtype=jnp.float32) / half_dim)
    angles = jnp.arange(length, dtype=jnp.float32)[:, None] * inverse[None, :]
    cosine = jnp.cos(angles)[:, None, :]
    sine_part = jnp.sin(angles)[:, None, :]
    lower_half = values[..., :half_dim]
    upper_half = values[..., half_dim:]
    return jnp.concatenate(
        [
            lower_half * cosine - upper_half * sine_part,
            upper_half * cosine + lower_half * sine_part,
        ],
        axis=-1,
    )


def carry_states(key_blocks, value_blocks, weighting, log_rates, block_size, backward):
    block_terms = jnp.einsum(
        "sbmhd,sbmhe->bshde",
        key_blocks * weighting[None, None, :, :, None],
        value_blocks,
        precision=highest_precision,
    )
    factor = jnp.exp(log_rates * block_size)[None, :, None, None]

    def advance(running, addend):
        return (running * factor + addend, running)

    initial = jnp.zeros(block_terms.shape[1:], jnp.float32)
    return lax.scan(advance, initial, block_terms, reverse=backward)[1]


def retain_blocks(
    query_rows, key_rows, value_rows, gate_rows, forward_decay, backward_decay, seq_count, length
):
    head_count = forward_decay.shape[0]
    head_dim = query_rows.shape[1] // head_count
    block_size = BLOCK
    block_count = length // block_size

    def split_heads(rows_in):
        return rows_in.astype(jnp.float32).reshape(seq_count, length, head_count, head_dim)

    def blocked(tensor):
        return tensor.reshape(seq_count, block_count, block_size, head_count, head_dim)

    queries = blocked(apply_rotary_heads(split_heads(query_rows), length))
    key_heads = blocked(apply_rotary_heads(split_heads(key_rows), length) * head_dim ** (-0.5))
    valued = blocked(split_heads(value_rows))
    rate_ahead = jax.nn.log_sigmoid(forward_decay)
    rate_behind = jax.nn.log_sigmoid(backward_decay)
    position = jnp.arange(block_size, dtype=jnp.float32)
    offset = position[:, None] - position[None, :]
    inside = jnp.where(
        offset[None] >= 0,
        jnp.exp(rate_ahead[:, None, None] * jnp.maximum(offset, 0.0)[None]),
        jnp.exp(rate_behind[:, None, None] * jnp.maximum(-offset, 0.0)[None]),
    )
    attention_scores = (
        jnp.einsum("sbchd,sbmhd->sbhcm", queries, key_heads, precision=highest_precision)
        * inside[None, None]
    )
    result = jnp.einsum("sbhcm,sbmhd->sbchd", attention_scores, valued, precision=highest_precision)
    column = position[:, None]
    key_ahead = jnp.exp(rate_ahead[None, :] * (block_size - 1 - column))
    query_ahead = jnp.exp(rate_ahead[None, :] * (column + 1))
    key_behind = jnp.exp(rate_behind[None, :] * column)
    query_behind = jnp.exp(rate_behind[None, :] * (block_size - column))
    from_before = carry_states(key_heads, valued, key_ahead, rate_ahead, block_size, False)
    from_after = carry_states(key_heads, valued, key_behind, rate_behind, block_size, True)
    result = (
        result
        + jnp.einsum("sbchd,bshde->sbche", queries, from_before, precision=highest_precision)
        * query_ahead[None, None, :, :, None]
    )
    result = (
        result
        + jnp.einsum("sbchd,bshde->sbche", queries, from_after, precision=highest_precision)
        * query_behind[None, None, :, :, None]
    )
    result = result.reshape(seq_count, length, head_count, head_dim)
    center = jnp.mean(result, axis=-1, keepdims=True)
    spread = jnp.mean(jnp.square(result - center), axis=-1, keepdims=True)
    normalized = (result - center) * lax.rsqrt(spread + group_eps)
    gated = jax.nn.silu(split_heads(gate_rows)) * normalized
    return gated.reshape(seq_count * length, head_count * head_dim).astype(jnp.bfloat16)


def accumulate(pieces, source):
    return tuple(
        (
            jnp.dot(source, weight_piece, preferred_element_type=jnp.float32)
            for weight_piece in pieces
        )
    )


def on_device(
    tokens,
    input_gain,
    query_weight,
    key_weight,
    value_weight,
    output_gate_matrix,
    forward_decay,
    backward_decay,
    merge_weight,
    middle_gain,
    gate_weight,
    up_weight,
    down_weight,
):
    seq_count, length, part_width = tokens.shape
    row_count = seq_count * length
    gathered = lax.all_gather(tokens, "tp", axis=2, tiled=True)
    normed = rms_scale(gathered.reshape(row_count, gathered.shape[2]), input_gain)
    query_sum, key_sum, value_sum, gating_sum = accumulate(
        (
            lax.all_gather(query_weight, "fs", axis=0, tiled=True),
            lax.all_gather(key_weight, "fs", axis=0, tiled=True),
            lax.all_gather(value_weight, "fs", axis=0, tiled=True),
            lax.all_gather(output_gate_matrix, "fs", axis=0, tiled=True),
        ),
        normed,
    )
    mixed = retain_blocks(
        query_sum.astype(jnp.bfloat16),
        key_sum.astype(jnp.bfloat16),
        value_sum.astype(jnp.bfloat16),
        gating_sum.astype(jnp.bfloat16),
        forward_decay,
        backward_decay,
        seq_count,
        length,
    )
    merge_term = jnp.dot(
        mixed,
        lax.all_gather(merge_weight, "fs", axis=1, tiled=True),
        preferred_element_type=jnp.float32,
    )
    merged = lax.psum_scatter(
        merge_term.astype(jnp.bfloat16), "tp", scatter_dimension=1, tiled=True
    ).astype(jnp.float32)
    middle = (tokens.reshape(row_count, part_width).astype(jnp.float32) + merged).astype(
        jnp.bfloat16
    )
    gathered_mid = lax.all_gather(middle, "tp", axis=1, tiled=True)
    normed_mid = rms_scale(gathered_mid, middle_gain)
    gate_full, up_full = (
        lax.all_gather(gate_weight, "fs", axis=0, tiled=True),
        lax.all_gather(up_weight, "fs", axis=0, tiled=True),
    )
    gate_act = jnp.dot(normed_mid, gate_full, preferred_element_type=jnp.float32)
    up_act = jnp.dot(normed_mid, up_full, preferred_element_type=jnp.float32)
    hidden = (jax.nn.silu(gate_act) * up_act).astype(jnp.bfloat16)
    down_term = jnp.dot(
        hidden,
        lax.all_gather(down_weight, "fs", axis=1, tiled=True),
        preferred_element_type=jnp.float32,
    )
    summed = lax.psum_scatter(
        down_term.astype(jnp.bfloat16), "tp", scatter_dimension=1, tiled=True
    ).astype(jnp.float32)
    layer_out = (middle.astype(jnp.float32) + summed).astype(jnp.bfloat16)
    return layer_out.reshape(seq_count, length, part_width)


def solution(mesh):
    placed = (
        P(("grp", "fs"), None, "tp"),
        P(),
        P("fs", "tp"),
        P("fs", "tp"),
        P("fs", "tp"),
        P("fs", "tp"),
        P("tp"),
        P("tp"),
        P("tp", "fs"),
        P(),
        P("fs", "tp"),
        P("fs", "tp"),
        P("tp", "fs"),
    )
    return jax.shard_map(
        on_device,
        mesh=mesh,
        in_specs=placed,
        out_specs=P(("grp", "fs"), None, "tp"),
        check_vma=False,
    )
```

profile of v0, /device:TPU:1, one launch (start us, length us, event | category | flops | bytes accessed | tf_op | source)
XLA Modules:
  0.0 570.7 jit_solution(758774433648440747)
XLA Ops:
  6.5 0.7 all-gather.11.cloned.1.call-update
  13.1 17.9 %all-gather.11.cloned.1.call-done = bf16[1,384,2048]{2,1,0:T(8,128)(2,1)} async-done(((bf16[1,384,512]{2,1,0:T(8,128)(2,1)}), bf16[1,384,2048]{2,1,0:T(8,128)(2,1)}) %all-gather.11.cloned.1.call-update) | async-done | bytes 1572880 | tf_op jit(solution)/shard_map/all_gather | solution.py:136
  31.0 1.9 fusion.3
  32.9 26.8 %all-gather.17.cloned.1.call-done = bf16[2048,256]{1,0:T(8,128)(2,1)} async-done(((bf16[512,256]{1,0:T(8,128)(2,1)}), bf16[2048,256]{1,0:T(8,128)(2,1)}) %all-gather.17.cloned.1.call-update) | async-done | bytes 1048592 | tf_op jit(solution)/shard_map/all_gather | solution.py:140
  59.7 2.6 convolution_convert_fusion.3
  62.3 26.4 %all-gather.19.cloned.1.call-done = bf16[2048,256]{1,0:T(8,128)(2,1)} async-done(((bf16[512,256]{1,0:T(8,128)(2,1)}), bf16[2048,256]{1,0:T(8,128)(2,1)}) %all-gather.19.cloned.1.call-update) | async-done | bytes 1048592 | tf_op jit(solution)/shard_map/all_gather | solution.py:141
  88.7 2.1 convolution_convert_fusion.2
  90.8 0.9 multiply_subtract_fusion.1
  91.9 1.7 concatenate.22
  93.6 1.0 pad_maximum_fusion
  94.8 22.7 %all-gather.15.cloned.1.call-done = bf16[2048,256]{1,0:T(8,128)(2,1)} async-done(((bf16[512,256]{1,0:T(8,128)(2,1)}), bf16[2048,256]{1,0:T(8,128)(2,1)}) %all-gather.15.cloned.1.call-update) | async-done | bytes 1048592 | tf_op jit(solution)/shard_map/all_gather | solution.py:142
  117.5 2.6 convolution_convert_fusion.4
  120.1 1.2 reshape.432
  123.6 0.8 fusion.9
  124.4 0.8 fusion.10
  125.2 1.4 convolution_multiply_fusion.1
  126.7 0.9 fusion.43
  127.9 1.2 reshape.431
  129.6 16.7 %all-gather.13.cloned.1.call-done = bf16[2048,256]{1,0:T(8,128)(2,1)} async-done(((bf16[512,256]{1,0:T(8,128)(2,1)}), bf16[2048,256]{1,0:T(8,128)(2,1)}) %all-gather.13.cloned.1.call-update) | async-done | bytes 1048592 | tf_op jit(solution)/shard_map/all_gather | solution.py:143
  146.3 28.8 %all-gather.21.cloned.1.call-done = bf16[256,2048]{1,0:T(8,128)(2,1)} async-done(((bf16[256,512]{1,0:T(8,128)(2,1)}), bf16[256,2048]{1,0:T(8,128)(2,1)}) %all-gather.21.cloned.1.call-update) | async-done | bytes 1048592 | tf_op jit(solution)/shard_map/all_gather | solution.py:159
  175.1 4.7 convolution_convert_fusion.1
  179.9 27.8 %reduce-scatter.3.cloned.1.call-done = bf16[384,512]{1,0:T(8,128)(2,1)} async-done(((bf16[384,2048]{1,0:T(8,128)(2,1)}), bf16[384,512]{1,0:T(8,128)(2,1)}) %reduce-scatter.3.cloned.1.call-update) | async-done | bytes 393232 | tf_op jit(solution)/shard_map/reduce_scatter | solution.py:162
  207.7 1.8 fusion.12
  211.9 18.1 %all-gather.23.cloned.1.call-done = bf16[384,2048]{1,0:T(8,128)(2,1)} async-done(((bf16[384,512]{1,0:T(8,128)(2,1)}), bf16[384,2048]{1,0:T(8,128)(2,1)}) %all-gather.23.cloned.1.call-update) | async-done | bytes 1572880 | tf_op jit(solution)/shard_map/all_gather | solution.py:168
  229.9 1.8 fusion
  231.7 97.5 %all-gather.25.cloned.1.call-done = bf16[2048,1280]{1,0:T(8,128)(2,1)} async-done(((bf16[512,1280]{1,0:T(8,128)(2,1)}), bf16[2048,1280]{1,0:T(8,128)(2,1)}) %all-gather.25.cloned.1.call-update) | async-done | bytes 5242896 | tf_op jit(solution)/shard_map/all_gather | solution.py:171
  329.2 6.5 %fusion.15 = f32[384,1280]{1,0:T(8,128)} fusion(bf16[2048,1280]{1,0:T(8,128)(2,1)} %all-gather.25.cloned.1.call-done, bf16[384,2048]{1,0:T(8,128)(2,1)} %all-gather.23.cloned.1.call-done, f32[2048]{0:T(1024)S(1)} %copy-done.12, f32[384]{0:T(512)S(1)} %add_rsqrt_fusion), kind=kOutput, calls=%fused_computation.36 | convolution fusion | flops 2016411648 | bytes 8791552 | tf_op jit(solution)/shard_map/dot_general | solution.py:174
  335.7 91.3 %all-gather.27.cloned.1.call-done = bf16[2048,1280]{1,0:T(8,128)(2,1)} async-done(((bf16[512,1280]{1,0:T(8,128)(2,1)}), bf16[2048,1280]{1,0:T(8,128)(2,1)}) %all-gather.27.cloned.1.call-update) | async-done | bytes 5242896 | tf_op jit(solution)/shard_map/all_gather | solution.py:172
  427.0 98.0 %all-gather.29.cloned.1.call-done = bf16[1280,2048]{1,0:T(8,128)(2,1)} async-done(((bf16[1280,512]{1,0:T(8,128)(2,1)}), bf16[1280,2048]{1,0:T(8,128)(2,1)}) %all-gather.29.cloned.1.call-update) | async-done | bytes 5242896 | tf_op jit(solution)/shard_map/all_gather | solution.py:179
  525.0 10.7 %convolution_convert_fusion = bf16[384,2048]{1,0:T(8,128)(2,1)} fusion(bf16[1280,2048]{1,0:T(8,128)(2,1)} %all-gather.29.cloned.1.call-done, bf16[2048,1280]{1,0:T(8,128)(2,1)} %all-gather.27.cloned.1.call-done, f32[384,1280]{1,0:T(8,128)} %fusion.15, bf16[384,2048]{1,0:T(8,128)(2,1)S(1)} %copy-done.3, f32[2048]{0:T(1024)S(1)} %copy-done.12, ...), kind=kOutput, calls=%fused_computation.15 | convolution fusion | flops 4033413120 | bytes 15607296 | tf_op jit(solution)/shard_map/dot_general | solution.py:177
  535.7 26.3 %reduce-scatter.5.cloned.1.call-done = bf16[384,512]{1,0:T(8,128)(2,1)} async-done(((bf16[384,2048]{1,0:T(8,128)(2,1)}), bf16[384,512]{1,0:T(8,128)(2,1)}) %reduce-scatter.5.cloned.1.call-update) | async-done | bytes 393232 | tf_op jit(solution)/shard_map/reduce_scatter | solution.py:182
  562.0 1.8 fusion.17
  (97 shorter events, 12.1 us)
Async XLA Ops:
  6.5 53.2 %copy-start.10 = (f32[2048]{0:T(1024)S(1)}, f32[2048]{0:T(1024)}, u32[]{:S(2)}) copy-start(f32[2048]{0:T(1024)} %param.18) | copy-start | bytes 24580
  6.5 24.5 %all-gather.11.cloned.1.call-start = ((), (), s32[]{:S(2)}) async-start(), calls=%async_computation.2 | async-start | bytes 1966080 | tf_op jit(solution)/shard_map/all_gather | solution.py:136
  7.3 52.5 %all-gather.17.cloned.1.call-start = ((), (), s32[]{:S(2)}) async-start(), calls=%async_computation.5 | async-start | bytes 1310720 | tf_op jit(solution)/shard_map/all_gather | solution.py:140
  8.0 80.7 %all-gather.19.cloned.1.call-start = ((), (), s32[]{:S(2)}) async-start(), calls=%async_computation.6 | async-start | bytes 1310720 | tf_op jit(solution)/shard_map/all_gather | solution.py:141
  8.7 108.8 %all-gather.15.cloned.1.call-start = ((), (), s32[]{:S(2)}) async-start(), calls=%async_computation.4 | async-start | bytes 1310720 | tf_op jit(solution)/shard_map/all_gather | solution.py:142
  9.3 137.0 %all-gather.13.cloned.1.call-start = ((), (), s32[]{:S(2)}) async-start(), calls=%async_computation.3 | async-start | bytes 1310720 | tf_op jit(solution)/shard_map/all_gather | solution.py:143
  9.9 165.2 %all-gather.21.cloned.1.call-start = ((), (), s32[]{:S(2)}) async-start(), calls=%async_computation.7 | async-start | bytes 1310720 | tf_op jit(solution)/shard_map/all_gather | solution.py:159
  10.5 197.2 %reduce-scatter.3.cloned.1.call-start = ((), (), s32[]{:S(2)}) async-start(), calls=%async_computation.8 | async-start | bytes 1966080 | tf_op jit(solution)/shard_map/reduce_scatter | solution.py:162
  31.0 57.7 %copy-start.1 = (bf16[1,384,2048]{2,1,0:T(8,128)(2,1)S(1)}, bf16[1,384,2048]{2,1,0:T(8,128)(2,1)}, u32[]{:S(2)}) copy-start(bf16[1,384,2048]{2,1,0:T(8,128)(2,1)} %all-gather.11.cloned.1.call-done) | copy-start | bytes 4718596
  32.9 57.9 %copy-start.8 = (f32[384]{0:T(512)}, f32[384]{0:T(512)S(1)}, u32[]{:S(2)}) copy-start(f32[384]{0:T(512)S(1)} %add_rsqrt_fusion.1) | copy-start | bytes 4612
  94.8 26.7 %copy-start.5 = (f32[3,128,4,32]{1,0,3,2:T(4,128)S(1)}, f32[3,128,4,32]{1,0,3,2:T(4,128)}, u32[]{:S(2)}) copy-start(f32[3,128,4,32]{1,0,3,2:T(4,128)} %concatenate.22) | copy-start | bytes 589828
  94.8 26.7 %copy-start.6 = (f32[128,4]{0,1:T(4,128)S(1)}, f32[128,4]{0,1:T(4,128)}, u32[]{:S(2)}) copy-start(f32[128,4]{0,1:T(4,128)} %get-tuple-element.231) | copy-start | bytes 6148
  94.8 26.7 %copy-start.7 = (f32[128,4]{0,1:T(4,128)S(1)}, f32[128,4]{0,1:T(4,128)}, u32[]{:S(2)}) copy-start(f32[128,4]{0,1:T(4,128)} %get-tuple-element.229) | copy-start | bytes 6148
  126.6 48.5 %copy-start.2 = (bf16[1,384,2048]{2,1,0:T(8,128)(2,1)S(1)}, bf16[1,384,2048]{2,1,0:T(8,128)(2,1)}, u32[]{:S(2)}) copy-start(bf16[1,384,2048]{2,1,0:T(8,128)(2,1)} %all-gather.11.cloned.1.call-done) | copy-start | bytes 4718596
  126.6 48.5 %copy-start.9 = (f32[384]{0:T(512)S(1)}, f32[384]{0:T(512)}, u32[]{:S(2)}) copy-start(f32[384]{0:T(512)} %copy-done.8) | copy-start | bytes 4612
  126.6 48.5 %copy-start.11 = (f32[2048]{0:T(1024)S(1)}, f32[2048]{0:T(1024)}, u32[]{:S(2)}) copy-start(f32[2048]{0:T(1024)} %param.18) | copy-start | bytes 24580
  129.6 78.1 %copy-start.4 = (bf16[1,384,512]{2,1,0:T(8,128)(2,1)S(1)}, bf16[1,384,512]{2,1,0:T(8,128)(2,1)}, u32[]{:S(2)}) copy-start(bf16[1,384,512]{2,1,0:T(8,128)(2,1)} %param.17) | copy-start | bytes 1179652
  179.9 50.1 %all-gather.23.cloned.1.call-start = ((), (), s32[]{:S(2)}) async-start(), calls=%async_computation.9 | async-start | bytes 1966080 | tf_op jit(solution)/shard_map/all_gather | solution.py:168
  209.5 119.7 %copy-start.12 = (f32[2048]{0:T(1024)S(1)}, f32[2048]{0:T(1024)}, u32[]{:S(2)}) copy-start(f32[2048]{0:T(1024)} %param.26) | copy-start | bytes 24580
  209.6 119.6 %all-gather.25.cloned.1.call-start = ((), (), s32[]{:S(2)}) async-start(), calls=%async_computation.10 | async-start | bytes 6553600 | tf_op jit(solution)/shard_map/all_gather | solution.py:171
  210.3 216.7 %all-gather.27.cloned.1.call-start = ((), (), s32[]{:S(2)}) async-start(), calls=%async_computation.11 | async-start | bytes 6553600 | tf_op jit(solution)/shard_map/all_gather | solution.py:172
  210.9 314.1 %all-gather.29.cloned.1.call-start = ((), (), s32[]{:S(2)}) async-start(), calls=%async_computation.12 | async-start | bytes 6553600 | tf_op jit(solution)/shard_map/all_gather | solution.py:179
  211.6 350.4 %reduce-scatter.5.cloned.1.call-start = ((), (), s32[]{:S(2)}) async-start(), calls=%async_computation.13 | async-start | bytes 1966080 | tf_op jit(solution)/shard_map/reduce_scatter | solution.py:182
  231.7 293.3 %copy-start.3 = (bf16[384,2048]{1,0:T(8,128)(2,1)S(1)}, bf16[384,2048]{1,0:T(8,128)(2,1)}, u32[]{:S(2)}) copy-start(bf16[384,2048]{1,0:T(8,128)(2,1)} %all-gather.23.cloned.1.call-done) | copy-start | bytes 4718596
  335.7 226.3 %copy-start = (bf16[384,512]{1,0:T(8,128)(2,1)S(1)}, bf16[384,512]{1,0:T(8,128)(2,1)}, u32[]{:S(2)}) copy-start(bf16[384,512]{1,0:T(8,128)(2,1)} %fusion.12) | copy-start | bytes 1179652
Sparse Core Ops, SparseCore 0:
  8.9 22.0 all-gather.10
  32.6 27.1 all-gather.16
  61.3 27.3 all-gather.18
  90.1 27.3 all-gather.14
  118.9 27.3 all-gather.12
  147.7 27.3 all-gather.20
  180.0 27.6 reduce-scatter.2
  209.7 20.1 all-gather.22
  231.5 97.6 all-gather.24
  330.6 96.3 all-gather.26
  428.6 96.3 all-gather.28
  535.8 26.1 reduce-scatter.4
where the time goes:
time: 572 us; the launch traced here: 571 us
  waiting for transfers between devices  504 us (88%)
  matrix products  33.9 us (6%)
  between operations  13.9 us (2%)
  other arithmetic  12.9 us (2%)
    all_gather x1, waiting for transfers between devices, on_device(): lax.all_gather(down_weight, 'fs', axis=1, tiled=True)  98 us
    all_gather x1, waiting for transfers between devices, on_device(): lax.all_gather(gate_weight, 'fs', axis=0, tiled=True)  97.5 us
    all_gather x1, waiting for transfers between devices, on_device(): lax.all_gather(up_weight, 'fs', axis=0, tiled=True)  91.3 us
    all_gather x1, waiting for transfers between devices, on_device(): lax.all_gather(merge_weight, 'fs', axis=1, tiled=True)  28.8 us
    reduce_scatter x1, waiting for transfers between devices, on_device(): lax.psum_scatter(merge_term.astype(jnp.bfloat16), 'tp', scatter_dimension...  27.8 us
    all_gather x1, waiting for transfers between devices, on_device(): lax.all_gather(query_weight, 'fs', axis=0, tiled=True)  26.8 us
    all_gather x1, waiting for transfers between devices, on_device(): lax.all_gather(key_weight, 'fs', axis=0, tiled=True)  26.4 us
    reduce_scatter x1, waiting for transfers between devices, on_device(): lax.psum_scatter(down_term.astype(jnp.bfloat16), 'tp', scatter_dimension=...  26.3 us
  transfers between devices with their start and end apart: 12, of which 12 were waited for; matrix products, arithmetic and copies ran while one was open for 6% of the time, Pallas kernels for 0%

commit v1 on v0

--- a/solution.py
+++ b/solution.py
@@ -1,6 +1,10 @@
+import functools
+
 import jax
 import jax.numpy as jnp
 from jax import lax
+from jax.experimental import pallas as pl
+from jax.experimental.pallas import tpu as pltpu
 from jax.sharding import PartitionSpec as P
 
 BLOCK = 128
@@ -107,16 +111,184 @@
     return gated.reshape(seq_count * length, head_count * head_dim).astype(jnp.bfloat16)
 
 
-def accumulate(pieces, source):
-    return tuple(
-        (
-            jnp.dot(source, weight_piece, preferred_element_type=jnp.float32)
-            for weight_piece in pieces
-        )
-    )
+MESH = pl.DeviceIdType.MESH
+
+
+def gather_kernel(sizes, *refs):
+    line, copies = sizes["fs"], sizes["grp"]
+    count = len(refs[:-5]) // 2
+    shards, slots = refs[:count], refs[count : 2 * count]
+    own_sem, line_send, line_recv, pair_send, pair_recv = refs[2 * count :]
+    place = lax.axis_index("fs")
+    half = lax.axis_index("grp")
+
+    barrier = pltpu.get_barrier_semaphore()
+    for shift in (1, -1):
+        there = place + shift
+
+        @pl.when((there >= 0) & (there < line))
+        def _():
+            pl.semaphore_signal(barrier, inc=1, device_id={"fs": there}, device_id_type=MESH)
+
+    for other in range(1, copies):
+        pl.semaphore_signal(
+            barrier,
+            inc=1,
+            device_id={"grp": lax.rem(half + other, copies)},
+            device_id_type=MESH,
+        )
+    own = [pltpu.make_async_copy(shards[k], slots[k].at[place], own_sem.at[k]) for k in range(count)]
+    for copy in own:
+        copy.start()
+    neighbours = (place > 0).astype(jnp.int32) + (place < line - 1).astype(jnp.int32)
+    pl.semaphore_wait(barrier, neighbours + copies - 1)
+
+    def piece(k, block, part):
+        rows = slots[k].shape[1] // copies
+        return slots[k].at[block, pl.ds(pl.multiple_of(part * rows, rows), rows), :]
+
+    def hop(k, way, step):
+        shift = 1 if way == 0 else -1
+        block = place - shift * step
+        return pltpu.make_async_remote_copy(
+            src_ref=piece(k, block, half),
+            dst_ref=piece(k, block, half),
+            send_sem=line_send.at[k, way, step],
+            recv_sem=line_recv.at[k, way, step],
+            device_id={"fs": place + shift},
+            device_id_type=MESH,
+        )
+
+    def arrival(k, way, step):
+        shift = 1 if way == 0 else -1
+        block = place - shift * step
+        return pltpu.make_async_remote_copy(
+            src_ref=piece(k, block, half),
+            dst_ref=piece(k, block, half),
+            send_sem=line_send.at[k, way, step - 1],
+            recv_sem=line_recv.at[k, way, step - 1],
+            device_id={"fs": place - shift},
+            device_id_type=MESH,
+        )
+
+    def across(k, way, step, other):
+        shift = 1 if way == 0 else -1
+        block = place - shift * step
+        return pltpu.make_async_remote_copy(
+            src_ref=piece(k, block, half),
+            dst_ref=piece(k, block, half),
+            send_sem=pair_send.at[k, way, step - 1, other - 1],
+            recv_sem=pair_recv.at[k, way, step - 1, other - 1],
+            device_id={"grp": lax.rem(half + other, copies)},
+            device_id_type=MESH,
+        )
+
+    def landed(k, way, step, other):
+        shift = 1 if way == 0 else -1
+        block = place - shift * step
+        source = lax.rem(half + copies - other, copies)
+        return pltpu.make_async_remote_copy(
+            src_ref=piece(k, block, source),
+            dst_ref=piece(k, block, source),
+            send_sem=pair_send.at[k, way, step - 1, other - 1],
+            recv_sem=pair_recv.at[k, way, step - 1, other - 1],
+            device_id={"grp": source},
+            device_id_type=MESH,
+        )
+
+    def has(way, step):
+        return place >= step if way == 0 else place + step < line
+
+    def goes(way):
+        return place < line - 1 if way == 0 else place > 0
+
+    def launch(k):
+        own[k].wait()
+        for way in range(2):
+
+            @pl.when(goes(way))
+            def _():
+                hop(k, way, 0).start()
+
+    def pump(k):
+        for step in range(1, line):
+            for way in range(2):
+
+                @pl.when(has(way, step))
+                def _():
+                    arrival(k, way, step).wait_recv()
+                    for other in range(1, copies):
+                        across(k, way, step, other).start()
+
+                @pl.when(has(way, step) & goes(way))
+                def _():
+                    hop(k, way, step).start()
+
+    def settle(k):
+        for step in range(1, line):
+            for way in range(2):
+
+                @pl.when(has(way, step))
+                def _():
+                    for other in range(1, copies):
+                        landed(k, way, step, other).wait_recv()
+
+    def drain(k):
+        for way in range(2):
+            for step in range(line):
+
+                @pl.when((has(way, step) if step else True) & goes(way))
+                def _():
+                    hop(k, way, step).wait_send()
+
+                if step:
+
+                    @pl.when(has(way, step))
+                    def _():
+                        for other in range(1, copies):
+                            across(k, way, step, other).wait_send()
+
+    for k in range(min(2, count)):
+        launch(k)
+    for k in range(count):
+        pump(k)
+        if k + 2 < count:
+            launch(k + 2)
+    for k in range(count):
+        settle(k)
+        drain(k)
+
+
+def gather_weights(sizes, shards):
+    line, copies, count = sizes["fs"], sizes["grp"], len(shards)
+    return pl.pallas_call(
+        functools.partial(gather_kernel, sizes),
+        out_shape=[jax.ShapeDtypeStruct((line,) + w.shape, w.dtype) for w in shards],
+        in_specs=[pl.BlockSpec(memory_space=pl.ANY)] * count,
+        out_specs=[pl.BlockSpec(memory_space=pltpu.VMEM)] * count,
+        scratch_shapes=[
+            pltpu.SemaphoreType.DMA((count,)),
+            pltpu.SemaphoreType.DMA((count, 2, line)),
+            pltpu.SemaphoreType.DMA((count, 2, line)),
+            pltpu.SemaphoreType.DMA((count, 2, line, copies - 1)),
+            pltpu.SemaphoreType.DMA((count, 2, line, copies - 1)),
+        ],
+        compiler_params=pltpu.CompilerParams(
+            collective_id=0, has_side_effects=True, vmem_limit_bytes=56 << 20
+        ),
+    )(*shards)
+
+
+def rows_of(blocks):
+    return blocks.reshape(-1, blocks.shape[2])
+
+
+def columns_of(blocks):
+    return blocks.transpose(1, 0, 2).reshape(blocks.shape[1], -1)
 
 
 def on_device(
+    sizes,
     tokens,
     input_gain,
     query_weight,
@@ -133,17 +305,16 @@
 ):
     seq_count, length, part_width = tokens.shape
     row_count = seq_count * length
+    joined = jnp.concatenate([query_weight, key_weight, value_weight, output_gate_matrix], axis=1)
+    joined_full, merge_full, gate_full, up_full, down_full = gather_weights(
+        sizes, (joined, merge_weight, gate_weight, up_weight, down_weight)
+    )
+    merge_full, down_full = columns_of(merge_full), columns_of(down_full)
+    gate_full, up_full = rows_of(gate_full), rows_of(up_full)
     gathered = lax.all_gather(tokens, "tp", axis=2, tiled=True)
     normed = rms_scale(gathered.reshape(row_count, gathered.shape[2]), input_gain)
-    query_sum, key_sum, value_sum, gating_sum = accumulate(
-        (
-            lax.all_gather(query_weight, "fs", axis=0, tiled=True),
-            lax.all_gather(key_weight, "fs", axis=0, tiled=True),
-            lax.all_gather(value_weight, "fs", axis=0, tiled=True),
-            lax.all_gather(output_gate_matrix, "fs", axis=0, tiled=True),
-        ),
-        normed,
-    )
+    projected = jnp.dot(normed, rows_of(joined_full), preferred_element_type=jnp.float32)
+    query_sum, key_sum, value_sum, gating_sum = jnp.split(projected, 4, axis=1)
     mixed = retain_blocks(
         query_sum.astype(jnp.bfloat16),
         key_sum.astype(jnp.bfloat16),
@@ -156,7 +327,7 @@
     )
     merge_term = jnp.dot(
         mixed,
-        lax.all_gather(merge_weight, "fs", axis=1, tiled=True),
+        merge_full,
         preferred_element_type=jnp.float32,
     )
     merged = lax.psum_scatter(
@@ -167,16 +338,12 @@
     )
     gathered_mid = lax.all_gather(middle, "tp", axis=1, tiled=True)
     normed_mid = rms_scale(gathered_mid, middle_gain)
-    gate_full, up_full = (
-        lax.all_gather(gate_weight, "fs", axis=0, tiled=True),
-        lax.all_gather(up_weight, "fs", axis=0, tiled=True),
-    )
     gate_act = jnp.dot(normed_mid, gate_full, preferred_element_type=jnp.float32)
     up_act = jnp.dot(normed_mid, up_full, preferred_element_type=jnp.float32)
     hidden = (jax.nn.silu(gate_act) * up_act).astype(jnp.bfloat16)
     down_term = jnp.dot(
         hidden,
-        lax.all_gather(down_weight, "fs", axis=1, tiled=True),
+        down_full,
         preferred_element_type=jnp.float32,
     )
     summed = lax.psum_scatter(
@@ -203,7 +370,7 @@
         P("tp", "fs"),
     )
     return jax.shard_map(
-        on_device,
+        functools.partial(on_device, dict(mesh.shape)),
         mesh=mesh,
         in_specs=placed,
         out_specs=P(("grp", "fs"), None, "tp"),

time: 572 us -> 351 us (0.61)
  waiting for transfers between devices: 504 us -> 70.2 us
  Pallas kernels: 0 us -> 208 us
  local copies, waits for them, and re-layouts: 5.45 us -> 13.3 us
    all_gather x8 -> x0, waiting for transfers between devices: 408 us -> none  [the longest x1 98 us: on_device(): lax.all_gather(down_weight, 'fs', axis=1, tiled=True)]
    pallas_call x0 -> x1, Pallas kernels: none -> 208 us  [gather_weights(): pl.pallas_call(functools.partial(gather_kernel, sizes), out_shape=[jax.Sh...]
    all_gather x1, waiting for transfers between devices: 17.9 us -> 0.01 us  [on_device(): gathered = lax.all_gather(tokens, 'tp', axis=2, tiled=True)]
    transpose x0 -> x2, local copies, waits for them, and re-layouts: none -> 9.35 us  [columns_of(): return blocks.transpose(1, 0, 2).reshape(blocks.shape[1], -1)]
    all_gather x1, waiting for transfers between devices: 18.1 us -> 12.2 us  [on_device(): gathered_mid = lax.all_gather(middle, 'tp', axis=1, tiled=True)]
    dot_general x5 -> x3, matrix products: 22.6 us -> 18 us  [the longest x1 10.7 us: on_device(): down_term = jnp.dot(hidden, down_full, preferred_element_type=jnp.float32)]
  transfers between devices with their start and end apart: 12 -> 4, of which waited for: 12 -> 3; matrix products, arithmetic and copies ran while one was open for 6% -> 4% of each run, Pallas kernels for 0% -> 59%
where the time goes in v1:
time: 351 us; the launch traced here: 350 us
  Pallas kernels  208 us (59%)
  waiting for transfers between devices  70.2 us (20%)
  matrix products  30.4 us (9%)
  other arithmetic  13.9 us (4%)
  between operations  13.5 us (4%)
  local copies, waits for them, and re-layouts  13.3 us (4%)
    pallas_call x1, Pallas kernels, gather_weights(): pl.pallas_call(functools.partial(gather_kernel, sizes), out_shape=[jax.Sh...  208 us
    reduce_scatter x1, waiting for transfers between devices, on_device(): lax.psum_scatter(merge_term.astype(jnp.bfloat16), 'tp', scatter_dimension...  29.6 us
    reduce_scatter x1, waiting for transfers between devices, on_device(): lax.psum_scatter(down_term.astype(jnp.bfloat16), 'tp', scatter_dimension=...  27.6 us
    all_gather x1, waiting for transfers between devices, on_device(): gathered_mid = lax.all_gather(middle, 'tp', axis=1, tiled=True)  12.2 us
    dot_general x1, matrix products, on_device(): down_term = jnp.dot(hidden, down_full, preferred_element_type=jnp.float32)  10.7 us
    transpose x2, local copies, waits for them, and re-layouts, columns_of(): return blocks.transpose(1, 0, 2).reshape(blocks.shape[1], -1)  9.35 us
  transfers between devices with their start and end apart: 4, of which 3 were waited for; matrix products, arithmetic and copies ran while one was open for 4% of the time, Pallas kernels for 59%

profile of v1, /device:TPU:1, one launch (start us, length us, event | category | flops | bytes accessed | tf_op | source)
XLA Modules:
  0.0 350.0 jit_solution(10120007702887955051)
XLA Ops:
  6.5 0.7 all-gather.3.cloned.1.call-update
  7.3 2.3 pad_maximum_fusion.refs_0_
  9.7 208.2 %shard_map.127 = (bf16[4,512,1024]{2,1,0:T(8,128)(2,1)}, bf16[4,256,512]{2,1,0:T(8,128)(2,1)}, bf16[4,512,1280]{2,1,0:T(8,128)(2,1)}, bf16[4,512,1280]{2,1,0:T(8,128)(2,1)}, bf16[4,1280,512]{2,1,0:T(8,128)(2,1)}) custom-call(bf16[512,1024]{1,0:T(8,128)(2,1)} %pad_maximum_fusion.refs_0_, bf16[256,512]{1,0:T(8,128)(2,1)} %refs_1_.1, ...), custom_call_target="tpu_custom_call" | custom-call | tf_op jit(solution)/shard_map/pallas_call | solution.py:264
  217.9 1.5 copy.40
  219.9 0.9 exponential_select_fusion
  220.8 1.8 fusion
  222.6 4.5 %fusion.12 = bf16[384,1024]{1,0:T(8,128)(2,1)S(1)} fusion(bf16[2048,1024]{1,0:T(8,128)(2,1)} %bitcast.118, bf16[1,384,2048]{2,1,0:T(8,128)(2,1)} %all-gather.3.cloned.1.call-done, f32[2048]{0:T(1024)S(1)} %copy-done.8, f32[384]{0:T(512)S(1)} %add_rsqrt_fusion.1), kind=kOutput, calls=%fused_computation.22 | convolution fusion | flops 1614151680 | bytes 6563328 | tf_op jit(solution)/shard_map/dot_general | solution.py:316
  227.2 0.8 copy-done.5
  228.4 0.9 multiply_subtract_fusion.1
  230.0 0.3 broadcast_multiply_fusion.2
  230.3 0.4 convolution_bitcast_fusion.3
  230.7 0.4 while.30
  231.1 0.7 copy-done.3
  231.9 1.0 pad_maximum_fusion.1
  233.1 0.4 convolution_bitcast_fusion.1
  233.6 0.4 while.31
  234.0 1.8 fusion.17
  235.8 0.8 fusion.18
  236.6 1.4 convolution_multiply_fusion.1
  238.1 0.9 fusion.52
  239.0 0.3 copy.45
  239.3 0.5 reshape.464
  240.3 2.7 convolution_convert_fusion.1
  243.1 29.6 %reduce-scatter.3.cloned.1.call-done = bf16[384,512]{1,0:T(8,128)(2,1)} async-done(((bf16[384,2048]{1,0:T(8,128)(2,1)}), bf16[384,512]{1,0:T(8,128)(2,1)}) %reduce-scatter.3.cloned.1.call-update) | async-done | bytes 393232 | tf_op jit(solution)/shard_map/reduce_scatter | solution.py:333
  272.7 1.8 fusion.19
  274.8 7.9 %copy.41 = bf16[1280,4,512]{0,2,1:T(8,128)(2,1)} copy(bf16[1280,4,512]{2,0,1:T(8,128)(2,1)} %bitcast.106) | data formatting | bytes 10485760 | tf_op jit(solution)/shard_map/transpose | solution.py:287
  282.6 12.2 %all-gather.5.cloned.1.call-done = bf16[384,2048]{1,0:T(8,128)(2,1)} async-done(((bf16[384,512]{1,0:T(8,128)(2,1)}), bf16[384,2048]{1,0:T(8,128)(2,1)}) %all-gather.5.cloned.1.call-update) | async-done | bytes 1572880 | tf_op jit(solution)/shard_map/all_gather | solution.py:339
  294.9 1.8 fusion.3
  296.7 6.6 %fusion.22 = f32[384,1280]{1,0:T(8,128)} fusion(bf16[2048,1280]{1,0:T(8,128)(2,1)} %bitcast.117, bf16[384,2048]{1,0:T(8,128)(2,1)} %all-gather.5.cloned.1.call-done, f32[2048]{0:T(1024)S(1)} %copy-done.9, f32[384]{0:T(512)S(1)} %add_rsqrt_fusion), kind=kOutput, calls=%fused_computation.39 | convolution fusion | flops 2016411648 | bytes 8791552 | tf_op jit(solution)/shard_map/dot_general | solution.py:341
  303.3 10.7 %convolution_convert_fusion = bf16[384,2048]{1,0:T(8,128)(2,1)} fusion(bf16[1280,2048]{0,1:T(8,128)(2,1)} %bitcast.107, bf16[2048,1280]{1,0:T(8,128)(2,1)} %bitcast.116, f32[384,1280]{1,0:T(8,128)} %fusion.22, bf16[384,2048]{1,0:T(8,128)(2,1)S(1)} %copy-done.1, f32[2048]{0:T(1024)S(1)} %copy-done.9, f32[384]{0:T(512)S(1)} %add_rsqrt_fusion), kind=kOutput, calls=%fused_computation.15 | convolution fusion | flops 4033413120 | bytes 15607296 | tf_op jit(solution)/shard_map/dot_general | solution.py:344
  314.1 27.6 %reduce-scatter.5.cloned.1.call-done = bf16[384,512]{1,0:T(8,128)(2,1)} async-done(((bf16[384,2048]{1,0:T(8,128)(2,1)}), bf16[384,512]{1,0:T(8,128)(2,1)}) %reduce-scatter.5.cloned.1.call-update) | async-done | bytes 393232 | tf_op jit(solution)/shard_map/reduce_scatter | solution.py:349
  341.7 1.8 fusion.28
  (70 shorter events, 3.3 us)
Async XLA Ops:
  6.5 214.3 %all-gather.3.cloned.1.call-start = ((), (), s32[]{:S(2)}) async-start(), calls=%async_computation.2 | async-start | bytes 1966080 | tf_op jit(solution)/shard_map/all_gather | solution.py:314
  7.3 265.4 %reduce-scatter.3.cloned.1.call-start = ((), (), s32[]{:S(2)}) async-start(), calls=%async_computation.3 | async-start | bytes 1966080 | tf_op jit(solution)/shard_map/reduce_scatter | solution.py:333
  217.8 1.6 copy-start.6
  217.8 1.6 copy-start.7
  217.8 4.8 %copy-start.8 = (f32[2048]{0:T(1024)S(1)}, f32[2048]{0:T(1024)}, u32[]{:S(2)}) copy-start(f32[2048]{0:T(1024)} %param.18) | copy-start | bytes 24580
  227.1 0.9 copy-start.5
  231.1 0.7 copy-start.3
  234.0 2.7 copy-start.4
  240.3 32.4 %copy-start.2 = (bf16[1,384,512]{2,1,0:T(8,128)(2,1)S(1)}, bf16[1,384,512]{2,1,0:T(8,128)(2,1)}, u32[]{:S(2)}) copy-start(bf16[1,384,512]{2,1,0:T(8,128)(2,1)} %param.17) | copy-start | bytes 1179652
  243.0 51.8 %all-gather.5.cloned.1.call-start = ((), (), s32[]{:S(2)}) async-start(), calls=%async_computation.4 | async-start | bytes 1966080 | tf_op jit(solution)/shard_map/all_gather | solution.py:339
  274.5 67.1 %reduce-scatter.5.cloned.1.call-start = ((), (), s32[]{:S(2)}) async-start(), calls=%async_computation.5 | async-start | bytes 1966080 | tf_op jit(solution)/shard_map/reduce_scatter | solution.py:349
  274.8 21.9 %copy-start.9 = (f32[2048]{0:T(1024)S(1)}, f32[2048]{0:T(1024)}, u32[]{:S(2)}) copy-start(f32[2048]{0:T(1024)} %param.26) | copy-start | bytes 24580
  296.7 6.6 %copy-start.1 = (bf16[384,2048]{1,0:T(8,128)(2,1)S(1)}, bf16[384,2048]{1,0:T(8,128)(2,1)}, u32[]{:S(2)}) copy-start(bf16[384,2048]{1,0:T(8,128)(2,1)} %all-gather.5.cloned.1.call-done) | copy-start | bytes 4718596
  303.3 38.3 %copy-start = (bf16[384,512]{1,0:T(8,128)(2,1)S(1)}, bf16[384,512]{1,0:T(8,128)(2,1)}, u32[]{:S(2)}) copy-start(bf16[384,512]{1,0:T(8,128)(2,1)} %fusion.19) | copy-start | bytes 1179652
Sparse Core Ops, SparseCore 0:
  8.9 22.0 all-gather.2
  243.2 29.4 reduce-scatter.2
  274.7 20.1 all-gather.4
  314.2 27.4 reduce-scatter.4

commit v2 on v1

v2 whole, which is shorter than its diff:
```python
import functools

import jax
import jax.numpy as jnp
from jax import lax
from jax.experimental import pallas as pl
from jax.experimental.pallas import tpu as pltpu
from jax.sharding import PartitionSpec as P

norm_eps = 1e-06
group_eps = 1e-05
rope_base = 10000.0


def turn_tables(length, head_dim, head_count):
    half_dim = head_dim // 2
    inverse = rope_base ** (-jnp.arange(half_dim, dtype=jnp.float32) / half_dim)
    angles = jnp.arange(length, dtype=jnp.float32)[:, None] * inverse[None, :]
    cosine, sine_part = jnp.cos(angles), jnp.sin(angles)
    return (
        jnp.tile(jnp.concatenate([cosine, cosine], axis=1), (1, head_count)),
        jnp.tile(jnp.concatenate([-sine_part, sine_part], axis=1), (1, head_count)),
    )


MESH = pl.DeviceIdType.MESH


def layer_kernel(
    sizes,
    tokens,
    input_gain,
    middle_gain,
    rate_ahead,
    rate_behind,
    cosine,
    sine_part,
    joined_shard,
    merge_shard,
    gate_shard,
    up_shard,
    down_shard,
    out,
    joined,
    merge,
    gate,
    up,
    down,
    gathered,
    gathered_mid,
    normed,
    projected,
    mixed,
    hidden,
    partial,
    received,
    partial_end,
    received_end,
    own_sem,
    line_send,
    line_recv,
    pair_send,
    pair_recv,
    row_send,
    row_recv,
    self_sem,
):
    line, copies, row = sizes["fs"], sizes["grp"], sizes["tp"]
    shards = (joined_shard, merge_shard, gate_shard, up_shard, down_shard)
    slots = (joined, merge, gate, up, down)
    count = len(slots)
    length, part_width = tokens.shape
    width = row * part_width
    seat = lax.axis_index("tp")
    place = lax.axis_index("fs")
    half = lax.axis_index("grp")

    barrier = pltpu.get_barrier_semaphore()
    for shift in (1, -1):
        there = place + shift

        @pl.when((there >= 0) & (there < line))
        def _():
            pl.semaphore_signal(barrier, inc=1, device_id={"fs": there}, device_id_type=MESH)

    for other in range(1, copies):
        pl.semaphore_signal(
            barrier,
            inc=1,
            device_id={"grp": lax.rem(half + other, copies)},
            device_id_type=MESH,
        )
    for other in range(1, row):
        pl.semaphore_signal(
            barrier,
            inc=1,
            device_id={"tp": lax.rem(seat + other, row)},
            device_id_type=MESH,
        )
    own = [pltpu.make_async_copy(shards[k], slots[k].at[place], own_sem.at[k]) for k in range(count)]
    for copy in own:
        copy.start()
    neighbours = (place > 0).astype(jnp.int32) + (place < line - 1).astype(jnp.int32)
    mine = pltpu.make_async_copy(tokens, gathered.at[seat], self_sem)
    mine.start()
    pl.semaphore_wait(barrier, neighbours + copies - 1 + row - 1)

    def piece(k, block, part):
        rows = slots[k].shape[1] // copies
        return slots[k].at[block, pl.ds(pl.multiple_of(part * rows, rows), rows), :]

    def hop(k, way, step):
        shift = 1 if way == 0 else -1
        block = place - shift * step
        return pltpu.make_async_remote_copy(
            src_ref=piece(k, block, half),
            dst_ref=piece(k, block, half),
            send_sem=line_send.at[k, way, step],
            recv_sem=line_recv.at[k, way, step],
            device_id={"fs": place + shift},
            device_id_type=MESH,
        )

    def arrival(k, way, step):
        shift = 1 if way == 0 else -1
        block = place - shift * step
        return pltpu.make_async_remote_copy(
            src_ref=piece(k, block, half),
            dst_ref=piece(k, block, half),
            send_sem=line_send.at[k, way, step - 1],
            recv_sem=line_recv.at[k, way, step - 1],
            device_id={"fs": place - shift},
            device_id_type=MESH,
        )

    def across(k, way, step, other):
        shift = 1 if way == 0 else -1
        block = place - shift * step
        return pltpu.make_async_remote_copy(
            src_ref=piece(k, block, half),
            dst_ref=piece(k, block, half),
            send_sem=pair_send.at[k, way, step - 1, other - 1],
            recv_sem=pair_recv.at[k, way, step - 1, other - 1],
            device_id={"grp": lax.rem(half + other, copies)},
            device_id_type=MESH,
        )

    def landed(k, way, step, other):
        shift = 1 if way == 0 else -1
        block = place - shift * step
        source = lax.rem(half + copies - other, copies)
        return pltpu.make_async_remote_copy(
            src_ref=piece(k, block, source),
            dst_ref=piece(k, block, source),
            send_sem=pair_send.at[k, way, step - 1, other - 1],
            recv_sem=pair_recv.at[k, way, step - 1, other - 1],
            device_id={"grp": source},
            device_id_type=MESH,
        )

    def has(way, step):
        return place >= step if way == 0 else place + step < line

    def goes(way):
        return place < line - 1 if way == 0 else place > 0

    def launch(k):
        own[k].wait()
        for way in range(2):

            @pl.when(goes(way))
            def _():
                hop(k, way, 0).start()

    def pump(k):
        for step in range(1, line):
            for way in range(2):

                @pl.when(has(way, step))
                def _():
                    arrival(k, way, step).wait_recv()
                    for other in range(1, copies):
                        across(k, way, step, other).start()

                @pl.when(has(way, step) & goes(way))
                def _():
                    hop(k, way, step).start()

    def settle(k):
        for step in range(1, line):
            for way in range(2):

                @pl.when(has(way, step))
                def _():
                    for other in range(1, copies):
                        landed(k, way, step, other).wait_recv()

    def drain(k):
        for way in range(2):
            for step in range(line):

                @pl.when((has(way, step) if step else True) & goes(way))
                def _():
                    hop(k, way, step).wait_send()

                if step:

                    @pl.when(has(way, step))
                    def _():
                        for other in range(1, copies):
                            across(k, way, step, other).wait_send()

    def spread(source, target, stage):
        return [
            pltpu.make_async_remote_copy(
                src_ref=source,
                dst_ref=target.at[seat],
                send_sem=row_send.at[stage, other - 1],
                recv_sem=row_recv.at[stage, other - 1],
                device_id={"tp": lax.rem(seat + other, row)},
                device_id_type=MESH,
            )
            for other in range(1, row)
        ]

    def spread_in(target, stage):
        sources = [lax.rem(seat + row - other, row) for other in range(1, row)]
        return [
            pltpu.make_async_remote_copy(
                src_ref=target.at[source],
                dst_ref=target.at[source],
                send_sem=row_send.at[stage, other],
                recv_sem=row_recv.at[stage, other],
                device_id={"tp": source},
                device_id_type=MESH,
            )
            for other, source in enumerate(sources)
        ]

    def scatter(source, target, stage, other):
        there = lax.rem(seat + other, row)
        return pltpu.make_async_remote_copy(
            src_ref=source.at[there],
            dst_ref=target.at[other - 1],
            send_sem=row_send.at[stage, other - 1],
            recv_sem=row_recv.at[stage, other - 1],
            device_id={"tp": there},
            device_id_type=MESH,
        )

    def normalize(source, gain_vector):
        total = jnp.zeros((length, 1), jnp.float32)
        for t in range(row):
            widened = source[t].astype(jnp.float32)
            total = total + jnp.sum(widened * widened, axis=1, keepdims=True)
        scale = lax.rsqrt(total / width + norm_eps)
        for t in range(row):
            span = slice(t * part_width, (t + 1) * part_width)
            scaled = source[t].astype(jnp.float32) * scale * gain_vector[:, span]
            normed[:, span] = scaled.astype(jnp.bfloat16)

    def times(weight, columns):
        block = weight[:, :, columns]
        return jnp.dot(
            normed[...], block.reshape(-1, block.shape[2]), preferred_element_type=jnp.float32
        )

    def shares(rows_in, weight, target):
        step = weight.shape[2]
        for block in range(line):
            term = jnp.dot(rows_in[...], weight[block], preferred_element_type=jnp.float32)
            begin = block * step
            inner = begin % part_width
            target[begin // part_width, :, inner : inner + step] = term.astype(jnp.bfloat16)

    launch(0)
    first = spread(tokens, gathered, 0)
    for copy in first:
        copy.start()
    launch(1)
    mine.wait()
    for copy in spread_in(gathered, 0):
        copy.wait_recv()
    normalize(gathered, input_gain)

    pump(0)
    launch(2)
    settle(0)
    ret_width = projected.shape[2]
    for t in range(4):
        projected[t] = (
            times(joined, slice(t * ret_width, (t + 1) * ret_width))
            .astype(jnp.bfloat16)
            .astype(jnp.float32)
        )
    pump(1)
    launch(3)

    head_count = rate_ahead.shape[0]
    head_dim = ret_width // head_count
    lane = lax.broadcasted_iota(jnp.int32, (length, ret_width), 1)
    in_lower = lax.rem(lane, head_dim) < head_dim // 2

    def turned(values):
        partner = jnp.where(
            in_lower,
            pltpu.roll(values, ret_width - head_dim // 2, 1),
            pltpu.roll(values, head_dim // 2, 1),
        )
        return values * cosine[...] + partner * sine_part[...]

    queries = turned(projected[0])
    key_heads = (turned(projected[1]) * head_dim ** (-0.5)).astype(jnp.bfloat16)
    valued = projected[2]
    offset = (
        lax.broadcasted_iota(jnp.int32, (length, length), 0)
        - lax.broadcasted_iota(jnp.int32, (length, length), 1)
    ).astype(jnp.float32)
    result = jnp.zeros((length, ret_width), jnp.float32)
    for h in range(head_count):
        here = (lane >= h * head_dim) & (lane < (h + 1) * head_dim)
        scores = lax.dot_general(
            jnp.where(here, queries, 0.0).astype(jnp.bfloat16),
            key_heads,
            (((1,), (1,)), ((), ())),
            preferred_element_type=jnp.float32,
        )
        decay = jnp.exp(jnp.where(offset >= 0, rate_ahead[h] * offset, -rate_behind[h] * offset))
        result = result + jnp.dot(
            (scores * decay).astype(jnp.bfloat16),
            jnp.where(here, valued, 0.0).astype(jnp.bfloat16),
            preferred_element_type=jnp.float32,
        )
    center = jnp.zeros((length, ret_width), jnp.float32)
    for h in range(head_count):
        here = (lane >= h * head_dim) & (lane < (h + 1) * head_dim)
        mean = jnp.sum(jnp.where(here, result, 0.0), axis=1, keepdims=True) / head_dim
        center = jnp.where(here, mean, center)
    centered = result - center
    squared = centered * centered
    factor = jnp.zeros((length, ret_width), jnp.float32)
    for h in range(head_count):
        here = (lane >= h * head_dim) & (lane < (h + 1) * head_dim)
        spread_h = jnp.sum(jnp.where(here, squared, 0.0), axis=1, keepdims=True) / head_dim
        factor = jnp.where(here, lax.rsqrt(spread_h + group_eps), factor)
    gates = projected[3]
    mixed[...] = (gates / (1.0 + jnp.exp(-gates)) * (centered * factor)).astype(jnp.bfloat16)

    settle(1)
    shares(mixed, merge, partial)
    for other in range(1, row):
        scatter(partial, received, 1, other).start()
    total = tokens[...].astype(jnp.float32) + partial[seat].astype(jnp.float32)
    for other in range(1, row):
        scatter(partial, received, 1, other).wait_recv()
        total = total + received[other - 1].astype(jnp.float32)
    gathered_mid[seat] = total.astype(jnp.bfloat16)
    second = spread(gathered_mid.at[seat], gathered_mid, 2)
    for copy in second:
        copy.start()
    pump(2)
    launch(4)
    for copy in spread_in(gathered_mid, 2):
        copy.wait_recv()
    normalize(gathered_mid, middle_gain)
    pump(3)
    settle(2)
    settle(3)
    hidden_width = hidden.shape[1]
    tile = 256 if hidden_width % 256 == 0 else 128

    @pl.loop(0, hidden_width // tile)
    def _(index):
        columns = pl.ds(pl.multiple_of(index * tile, tile), tile)
        gate_act = times(gate, columns)
        up_act = times(up, columns)
        hidden[:, columns] = (gate_act / (1.0 + jnp.exp(-gate_act)) * up_act).astype(jnp.bfloat16)

    pump(4)
    settle(4)
    shares(hidden, down, partial_end)
    for other in range(1, row):
        scatter(partial_end, received_end, 3, other).start()
    total = gathered_mid[seat].astype(jnp.float32) + partial_end[seat].astype(jnp.float32)
    for other in range(1, row):
        scatter(partial_end, received_end, 3, other).wait_recv()
        total = total + received_end[other - 1].astype(jnp.float32)
    out[...] = total.astype(jnp.bfloat16)
    for copy in first + second:
        copy.wait_send()
    for other in range(1, row):
        scatter(partial, received, 1, other).wait_send()
        scatter(partial_end, received_end, 3, other).wait_send()
    for k in range(count):
        drain(k)


def on_device(
    sizes,
    tokens,
    input_gain,
    query_weight,
    key_weight,
    value_weight,
    output_gate_matrix,
    forward_decay,
    backward_decay,
    merge_weight,
    middle_gain,
    gate_weight,
    up_weight,
    down_weight,
):
    seq_count, length, part_width = tokens.shape
    flat = tokens.reshape(seq_count * length, part_width)
    joined = jnp.concatenate([query_weight, key_weight, value_weight, output_gate_matrix], axis=1)
    shards = (joined, merge_weight, gate_weight, up_weight, down_weight)
    line, copies, row, count = sizes["fs"], sizes["grp"], sizes["tp"], len(shards)
    width, ret_width, hidden_width = row * part_width, query_weight.shape[1], gate_weight.shape[1]
    head_count = forward_decay.shape[0]
    tables = turn_tables(length, ret_width // head_count, head_count)
    in_vmem = pl.BlockSpec(memory_space=pltpu.VMEM)
    in_smem = pl.BlockSpec(memory_space=pltpu.SMEM)
    bf16 = jnp.bfloat16
    layer_out = pl.pallas_call(
        functools.partial(layer_kernel, sizes),
        out_shape=jax.ShapeDtypeStruct(flat.shape, bf16),
        in_specs=[in_vmem] * 3
        + [in_smem] * 2
        + [in_vmem] * 2
        + [pl.BlockSpec(memory_space=pl.ANY)] * count,
        out_specs=in_vmem,
        scratch_shapes=[pltpu.VMEM((line,) + w.shape, w.dtype) for w in shards]
        + [
            pltpu.VMEM((row, length, part_width), bf16),
            pltpu.VMEM((row, length, part_width), bf16),
            pltpu.VMEM((length, width), bf16),
            pltpu.VMEM((4, length, ret_width), jnp.float32),
            pltpu.VMEM((length, ret_width), bf16),
            pltpu.VMEM((length, hidden_width), bf16),
            pltpu.VMEM((row, length, part_width), bf16),
            pltpu.VMEM((row - 1, length, part_width), bf16),
            pltpu.VMEM((row, length, part_width), bf16),
            pltpu.VMEM((row - 1, length, part_width), bf16),
            pltpu.SemaphoreType.DMA((count,)),
            pltpu.SemaphoreType.DMA((count, 2, line)),
            pltpu.SemaphoreType.DMA((count, 2, line)),
            pltpu.SemaphoreType.DMA((count, 2, line, copies - 1)),
            pltpu.SemaphoreType.DMA((count, 2, line, copies - 1)),
            pltpu.SemaphoreType.DMA((4, row - 1)),
            pltpu.SemaphoreType.DMA((4, row - 1)),
            pltpu.SemaphoreType.DMA,
        ],
        compiler_params=pltpu.CompilerParams(
            collective_id=0, has_side_effects=True, vmem_limit_bytes=58 << 20
        ),
    )(
        flat,
        input_gain[None, :],
        middle_gain[None, :],
        jax.nn.log_sigmoid(forward_decay),
        jax.nn.log_sigmoid(backward_decay),
        *tables,
        *shards,
    )
    return layer_out.reshape(seq_count, length, part_width)


def solution(mesh):
    placed = (
        P(("grp", "fs"), None, "tp"),
        P(),
        P("fs", "tp"),
        P("fs", "tp"),
        P("fs", "tp"),
        P("fs", "tp"),
        P("tp"),
        P("tp"),
        P("tp", "fs"),
        P(),
        P("fs", "tp"),
        P("fs", "tp"),
        P("tp", "fs"),
    )
    return jax.shard_map(
        functools.partial(on_device, dict(mesh.shape)),
        mesh=mesh,
        in_specs=placed,
        out_specs=P(("grp", "fs"), None, "tp"),
        check_vma=False,
    )
```

time: 351 us -> 241 us (0.69)
  waiting for transfers between devices: 70.2 us -> 0 us
  matrix products: 30.4 us -> 0 us
  Pallas kernels: 208 us -> 234 us
  between operations: 13.5 us -> 0.07 us
  other arithmetic: 13.9 us -> 2.67 us
  local copies, waits for them, and re-layouts: 13.3 us -> 3.69 us
    reduce_scatter x2 -> x0, waiting for transfers between devices: 57.2 us -> none  [the longest x1 29.6 us: on_device(): lax.psum_scatter(merge_term.astype(jnp.bfloat16), 'tp', scatter_dimension...]
    dot_general x10 -> x0, matrix products: 30.4 us -> none  [the longest x1 10.7 us: on_device(): down_term = jnp.dot(hidden, down_full, preferred_element_type=jnp.float32)]
    pallas_call x1, Pallas kernels: 208 us -> 234 us  [on_device(): pl.pallas_call(functools.partial(layer_kernel, sizes), out_shape=jax.Shap...]
    all_gather x2 -> x0, waiting for transfers between devices: 12.2 us -> none  [the longest x1 12.2 us: on_device(): gathered_mid = lax.all_gather(middle, 'tp', axis=1, tiled=True)]
    transpose x2 -> x0, local copies, waits for them, and re-layouts: 9.35 us -> none  [columns_of(): return blocks.transpose(1, 0, 2).reshape(blocks.shape[1], -1)]
    reduce_sum x3 -> x0, other arithmetic: 3.65 us -> none  [the longest x2 3.58 us: rms_scale(): jnp.mean(widened * widened, axis=-1, keepdims=True) + norm_eps]
  transfers between devices with their start and end apart: 4 -> 0, of which waited for: 3 -> 0; matrix products, arithmetic and copies ran while one was open for 4% -> 0% of each run, Pallas kernels for 59% -> 0%
where the time goes in v2:
time: 241 us
  Pallas kernels  234 us (97%)
  local copies, waits for them, and re-layouts  3.69 us (2%)
  other arithmetic  2.67 us (1%)
    pallas_call x1, Pallas kernels, on_device(): pl.pallas_call(functools.partial(layer_kernel, sizes), out_shape=jax.Shap...  234 us

profile of v2, /device:TPU:1, one launch (start us, length us, event | category | flops | bytes accessed | tf_op | source)
XLA Modules:
  0.0 240.8 jit_solution(17028503223091168695)
XLA Ops:
  0.0 1.3 fusion.3
  1.3 0.3 fusion.2
  1.6 0.0 copy-start
  1.6 0.0 copy-start.1
  1.6 0.0 copy-start.2
  1.6 0.0 copy-start.3
  1.7 0.9 copy.14.cosine
  2.6 0.9 copy.15.sine_part
  3.5 0.0 copy-done
  3.5 0.0 copy-done.1
  3.5 0.0 copy-done.2
  3.5 0.0 copy-done.3
  3.5 1.1 pad_maximum_fusion.joined_shard
  4.7 234.3 %shard_map.127 = bf16[384,512]{1,0:T(8,128)(2,1)} custom-call(bf16[384,512]{1,0:T(8,128)(2,1)} %bitcast.9, f32[1,2048]{1,0:T(1,128)} %bitcast.10, f32[1,2048]{1,0:T(1,128)} %bitcast.11, f32[4]{0:T(128)} %get-tuple-element.10.rate_ahead, f32[4]{0:T(128)} %get-tuple-element.11.rate_behind, f32[384,256]{1,0:T(8,128)} %copy.14.cosine, ...), custom_call_target="tpu_custom_call" | custom-call | tf_op jit(solution)/shard_map/pallas_call | solution.py:425
  239.0 1.8 copy.17
  (4 shorter events, 0.1 us)
Async XLA Ops:
  1.6 2.0 copy-start
  1.6 2.0 copy-start.1
  1.6 1.9 copy-start.2
  1.6 1.9 copy-start.3

commit v3 on v2

--- a/solution.py
+++ b/solution.py
@@ -2,6 +2,7 @@
 
 import jax
 import jax.numpy as jnp
+import numpy as np
 from jax import lax
 from jax.experimental import pallas as pl
 from jax.experimental.pallas import tpu as pltpu
@@ -14,12 +15,12 @@
 
 def turn_tables(length, head_dim, head_count):
     half_dim = head_dim // 2
-    inverse = rope_base ** (-jnp.arange(half_dim, dtype=jnp.float32) / half_dim)
-    angles = jnp.arange(length, dtype=jnp.float32)[:, None] * inverse[None, :]
-    cosine, sine_part = jnp.cos(angles), jnp.sin(angles)
+    inverse = rope_base ** (-np.arange(half_dim) / half_dim)
+    angles = np.arange(length)[:, None] * inverse[None, :]
+    cosine, sine_part = np.cos(angles), np.sin(angles)
     return (
-        jnp.tile(jnp.concatenate([cosine, cosine], axis=1), (1, head_count)),
-        jnp.tile(jnp.concatenate([-sine_part, sine_part], axis=1), (1, head_count)),
+        np.tile(np.concatenate([cosine, cosine], axis=1), (1, head_count)).astype(np.float32),
+        np.tile(np.concatenate([-sine_part, sine_part], axis=1), (1, head_count)).astype(np.float32),
     )
 
 
@@ -45,29 +46,35 @@
     merge,
     gate,
     up,
-    down,
-    gathered,
-    gathered_mid,
-    normed,
-    projected,
-    mixed,
-    hidden,
-    partial,
-    received,
-    partial_end,
-    received_end,
-    own_sem,
-    line_send,
-    line_recv,
-    pair_send,
-    pair_recv,
-    row_send,
-    row_recv,
-    self_sem,
+    *rest,
 ):
     line, copies, row = sizes["fs"], sizes["grp"], sizes["tp"]
-    shards = (joined_shard, merge_shard, gate_shard, up_shard, down_shard)
-    slots = (joined, merge, gate, up, down)
+    parts = len(rest) - 18
+    downs, partial_ends, received_ends = rest[:parts], rest[-2], rest[-1]
+    (
+        gathered,
+        gathered_mid,
+        normed,
+        projected,
+        mixed,
+        hidden,
+        partial,
+        received,
+        own_sem,
+        line_send,
+        line_recv,
+        pair_send,
+        pair_recv,
+        row_send,
+        row_recv,
+        self_sem,
+    ) = rest[parts:-2]
+    piece_width = downs[0].shape[2]
+    shards = (joined_shard, merge_shard, gate_shard, up_shard) + tuple(
+        down_shard if parts == 1 else down_shard.at[:, pl.ds(i * piece_width, piece_width)]
+        for i in range(parts)
+    )
+    slots = (joined, merge, gate, up) + tuple(downs)
     count = len(slots)
     length, part_width = tokens.shape
     width = row * part_width
@@ -272,6 +279,31 @@
             begin = block * step
             inner = begin % part_width
             target[begin // part_width, :, inner : inner + step] = term.astype(jnp.bfloat16)
+
+    def finish(i):
+        settle(4 + i)
+        if parts == 1:
+            shares(hidden, downs[i], partial_ends.at[i])
+        else:
+            for j in range(row):
+                blocks = [jnp.dot(
+                    hidden[...], downs[i][j * line // row + c], preferred_element_type=jnp.float32
+                ) for c in range(max(1, line // row))]
+                for c, term in enumerate(blocks):
+                    partial_ends[i, j, :, c * piece_width : (c + 1) * piece_width] = term.astype(
+                        jnp.bfloat16
+                    )
+        for other in range(1, row):
+            scatter(partial_ends.at[i], received_ends.at[i], 3 + i, other).start()
+
+    def collect(i):
+        span = slice(None) if parts == 1 else slice(i * piece_width, (i + 1) * piece_width)
+        total = gathered_mid[seat, :, span].astype(jnp.float32)
+        total = total + partial_ends[i, seat].astype(jnp.float32)
+        for other in range(1, row):
+            scatter(partial_ends.at[i], received_ends.at[i], 3 + i, other).wait_recv()
+            total = total + received_ends[i, other - 1].astype(jnp.float32)
+        out[:, span] = total.astype(jnp.bfloat16)
 
     launch(0)
     first = spread(tokens, gathered, 0)
@@ -350,6 +382,7 @@
     shares(mixed, merge, partial)
     for other in range(1, row):
         scatter(partial, received, 1, other).start()
+    pump(2)
     total = tokens[...].astype(jnp.float32) + partial[seat].astype(jnp.float32)
     for other in range(1, row):
         scatter(partial, received, 1, other).wait_recv()
@@ -358,12 +391,13 @@
     second = spread(gathered_mid.at[seat], gathered_mid, 2)
     for copy in second:
         copy.start()
-    pump(2)
+    pump(3)
     launch(4)
+    if parts > 1:
+        launch(5)
     for copy in spread_in(gathered_mid, 2):
         copy.wait_recv()
     normalize(gathered_mid, middle_gain)
-    pump(3)
     settle(2)
     settle(3)
     hidden_width = hidden.shape[1]
@@ -376,21 +410,21 @@
         up_act = times(up, columns)
         hidden[:, columns] = (gate_act / (1.0 + jnp.exp(-gate_act)) * up_act).astype(jnp.bfloat16)
 
-    pump(4)
-    settle(4)
-    shares(hidden, down, partial_end)
-    for other in range(1, row):
-        scatter(partial_end, received_end, 3, other).start()
-    total = gathered_mid[seat].astype(jnp.float32) + partial_end[seat].astype(jnp.float32)
-    for other in range(1, row):
-        scatter(partial_end, received_end, 3, other).wait_recv()
-        total = total + received_end[other - 1].astype(jnp.float32)
-    out[...] = total.astype(jnp.bfloat16)
+    for i in range(parts):
+        pump(4 + i)
+        if i + 2 < parts:
+            launch(6 + i)
+        if i:
+            finish(i - 1)
+    finish(parts - 1)
+    for i in range(parts):
+        collect(i)
     for copy in first + second:
         copy.wait_send()
     for other in range(1, row):
         scatter(partial, received, 1, other).wait_send()
-        scatter(partial_end, received_end, 3, other).wait_send()
+        for i in range(parts):
+            scatter(partial_ends.at[i], received_ends.at[i], 3 + i, other).wait_send()
     for k in range(count):
         drain(k)
 
@@ -415,7 +449,12 @@
     flat = tokens.reshape(seq_count * length, part_width)
     joined = jnp.concatenate([query_weight, key_weight, value_weight, output_gate_matrix], axis=1)
     shards = (joined, merge_weight, gate_weight, up_weight, down_weight)
-    line, copies, row, count = sizes["fs"], sizes["grp"], sizes["tp"], len(shards)
+    line, copies, row = sizes["fs"], sizes["grp"], sizes["tp"]
+    down_width = down_weight.shape[1]
+    parts = down_width // 256 if line == row and down_width % 256 == 0 else 1
+    down_piece = jax.ShapeDtypeStruct((down_weight.shape[0], down_width // parts), jnp.bfloat16)
+    landing = shards[:4] + (down_piece,) * parts
+    count = len(landing)
     width, ret_width, hidden_width = row * part_width, query_weight.shape[1], gate_weight.shape[1]
     head_count = forward_decay.shape[0]
     tables = turn_tables(length, ret_width // head_count, head_count)
@@ -428,9 +467,9 @@
         in_specs=[in_vmem] * 3
         + [in_smem] * 2
         + [in_vmem] * 2
-        + [pl.BlockSpec(memory_space=pl.ANY)] * count,
+        + [pl.BlockSpec(memory_space=pl.ANY)] * len(shards),
         out_specs=in_vmem,
-        scratch_shapes=[pltpu.VMEM((line,) + w.shape, w.dtype) for w in shards]
+        scratch_shapes=[pltpu.VMEM((line,) + w.shape, w.dtype) for w in landing]
         + [
             pltpu.VMEM((row, length, part_width), bf16),
             pltpu.VMEM((row, length, part_width), bf16),
@@ -440,16 +479,16 @@
             pltpu.VMEM((length, hidden_width), bf16),
             pltpu.VMEM((row, length, part_width), bf16),
             pltpu.VMEM((row - 1, length, part_width), bf16),
-            pltpu.VMEM((row, length, part_width), bf16),
-            pltpu.VMEM((row - 1, length, part_width), bf16),
             pltpu.SemaphoreType.DMA((count,)),
             pltpu.SemaphoreType.DMA((count, 2, line)),
             pltpu.SemaphoreType.DMA((count, 2, line)),
             pltpu.SemaphoreType.DMA((count, 2, line, copies - 1)),
             pltpu.SemaphoreType.DMA((count, 2, line, copies - 1)),
-            pltpu.SemaphoreType.DMA((4, row - 1)),
-            pltpu.SemaphoreType.DMA((4, row - 1)),
+            pltpu.SemaphoreType.DMA((3 + parts, row - 1)),
+            pltpu.SemaphoreType.DMA((3 + parts, row - 1)),
             pltpu.SemaphoreType.DMA,
+            pltpu.VMEM((parts, row, length, part_width // parts), bf16),
+            pltpu.VMEM((parts, row - 1, length, part_width // parts), bf16),
         ],
         compiler_params=pltpu.CompilerParams(
             collective_id=0, has_side_effects=True, vmem_limit_bytes=58 << 20

time: 241 us -> 220 us (0.913)
  Pallas kernels: 234 us -> 214 us
    pallas_call x1, Pallas kernels: 234 us -> 214 us  [on_device(): pl.pallas_call(functools.partial(layer_kernel, sizes), out_shape=jax.Shap...]
where the time goes in v3:
time: 220 us; the launch traced here: 219 us
  Pallas kernels  214 us (97%)
  other arithmetic  3.59 us (2%)
    pallas_call x1, Pallas kernels, on_device(): pl.pallas_call(functools.partial(layer_kernel, sizes), out_shape=jax.Shap...  214 us

profile of v3, /device:TPU:1, one launch (start us, length us, event | category | flops | bytes accessed | tf_op | source)
XLA Modules:
  0.0 219.4 jit_solution(5298518211976847505)
XLA Ops:
  0.0 1.3 fusion
  1.3 2.3 %pad_maximum_fusion.joined_shard = bf16[512,1024]{1,0:T(8,128)(2,1)} fusion(bf16[512,256]{1,0:T(8,128)(2,1)} %param.20, bf16[512,256]{1,0:T(8,128)(2,1)} %param.19, bf16[512,256]{1,0:T(8,128)(2,1)} %param.18, bf16[512,256]{1,0:T(8,128)(2,1)} %param.17), kind=kLoop, calls=%fused_computation | loop fusion | flops 4194304 | bytes 2097152 | tf_op jit(solution)/shard_map/concatenate | solution.py:450
  3.6 214.1 %shard_map.145 = bf16[384,512]{1,0:T(8,128)(2,1)} custom-call(bf16[384,512]{1,0:T(8,128)(2,1)} %bitcast.5, f32[1,2048]{1,0:T(1,128)} %bitcast.6, f32[1,2048]{1,0:T(1,128)} %bitcast.7, f32[4]{0:T(128)} %get-tuple-element.5.rate_ahead, f32[4]{0:T(128)} %get-tuple-element.6.rate_behind, f32[384,256]{1,0:T(8,128)} %constant.9.clone.cosine, ...), custom_call_target="tpu_custom_call" | custom-call | tf_op jit(solution)/shard_map/pallas_call | solution.py:464
  217.7 1.8 copy.17
